TPU v7x, 256 devices: a 4x2x16 block of a 4x16x16 slice. The times are simulated.
256 devices in a mesh: grp: 2 (over y), fs: 16 (over z), tp: 8 (over x, core).
Axes of the slice: x: 4, y: 2, z: 16, core: 2. Of those that a mesh axis runs over, the one named last changes fastest.
The devices are a block of a 4x16x16 slice.
Arguments:
- tokens: bfloat16 [32768, 2048], P(('grp', 'fs', 'tp')), parts along dimension 0, may hold values from -12 to 12
- norm_gain: float32 [2048], replicated, may hold values from 0.1 to 1.9
- w_in: bfloat16 [2048, 8192], P('fs', 'tp'), may hold values from -0.125 to 0.125
- w_out: bfloat16 [8192, 2048], P('tp', 'fs'), may hold values from -0.0625 to 0.0625
Outputs:
- mixed: bfloat16 [32768, 2048], P(('grp', 'fs', 'tp')), parts along dimension 0
There are 2 independent parts, one for each index of `grp`. A program takes and returns all parts, laid end to end along the dimension named above; an argument that names none is the same for every part. Nothing has to cross between parts.
All inputs are finite; a program needn't handle non-finite values.
Results may differ from a plain program's by a relative error of at most 0.012.
Values may be sent and summed in bfloat16 or wider, within the bound.
No kernel may reach another device: no remote copies, remote signals or barrier semaphores. Data moves between devices by JAX's collectives and lax.ppermute only.
A program may use at most 64 MiB of HBM per device.

v0:
```python
import jax
import jax.numpy as jnp
from jax import lax
from jax.sharding import PartitionSpec as P

EPS = 1e-06


def from_everyone(shard, axis):
    copies = jnp.broadcast_to(shard, (lax.axis_size(axis), *shard.shape))
    return lax.all_to_all(copies, axis, split_axis=0, concat_axis=0, tiled=True)


def joined_along(parts, dim):
    parts = jnp.moveaxis(parts, 0, dim)
    shape = parts.shape
    return parts.reshape(*shape[:dim], shape[dim] * shape[dim + 1], *shape[dim + 2 :])


def collect(shard, axis, dim):
    parts = from_everyone(shard, axis)
    return joined_along(parts, dim)


def local(tokens, norm_gain, w_in, w_out):
    xf = tokens.astype(jnp.float32)
    scale = lax.rsqrt(jnp.mean(xf * xf, axis=-1, keepdims=True) + EPS)
    normed = (xf * scale * norm_gain).astype(jnp.bfloat16)
    whole_in = lax.all_gather(w_in, "fs", axis=0, tiled=True)
    pre = jnp.dot(collect(normed, "tp", 0), whole_in, preferred_element_type=jnp.float32)
    hidden = jnp.square(jax.nn.relu(pre)).astype(jnp.bfloat16)
    whole_out = lax.all_gather(w_out, "fs", axis=1, tiled=True)
    summed = lax.psum_scatter(
        jnp.dot(hidden, whole_out, preferred_element_type=jnp.float32).astype(jnp.bfloat16),
        "tp",
        scatter_dimension=0,
        tiled=True,
    ).astype(jnp.float32)
    return (xf + summed).astype(jnp.bfloat16)


def solution(mesh):
    in_specs = (P(("grp", "fs", "tp"), None), P(), P("fs", "tp"), P("tp", "fs"))
    out_specs = P(("grp", "fs", "tp"), None)
    return jax.shard_map(local, mesh=mesh, in_specs=in_specs, out_specs=out_specs, check_vma=False)
```

profile of v0, /device:TPU:40, one launch (start us, length us, event | category | flops | bytes accessed | tf_op | source)
XLA Modules:
  0.0 253.1 jit_solution(16195759570042781914)
XLA Ops:
  6.5 0.0 all-gather.3.cloned.1.call-start
  6.6 0.7 all-gather.3.cloned.1.call-update
  7.3 0.1 all-gather.5.cloned.1.call-start
  7.4 0.7 all-gather.5.cloned.1.call-update
  8.1 0.1 reduce-scatter.2.cloned.1.call-start
  8.2 1.2 fusion
  9.4 1.2 fusion.2
  10.7 0.5 broadcast_in_dim.2
  11.2 54.2 %all_to_all.5 = bf16[8,128,2048]{2,1,0:T(8,128)(2,1)} all-to-all(bf16[8,128,2048]{2,1,0:T(8,128)(2,1)S(1)} %broadcast_in_dim.2), channel_id=1, replica_groups=mesh['grp'=2,'fs'=16,'tp'=8] {'tp'}, dimensions={0} | all-to-all | bytes 8388608 | tf_op jit(solution)/shard_map/all_to_all | solution.py:11
  65.4 33.0 %all-gather.3.cloned.1.call-done = bf16[2048,1024]{1,0:T(8,128)(2,1)} async-done(((bf16[128,1024]{1,0:T(8,128)(2,1)}), bf16[2048,1024]{1,0:T(8,128)(2,1)}) %all-gather.3.cloned.1.call-update) | async-done | bytes 4194320 | tf_op jit(solution)/shard_map/all_gather | solution.py:29
  98.3 91.3 %all-gather.5.cloned.1.call-done = bf16[1024,2048]{1,0:T(8,128)(2,1)} async-done(((bf16[1024,128]{1,0:T(8,128)(2,1)}), bf16[1024,2048]{1,0:T(8,128)(2,1)}) %all-gather.5.cloned.1.call-update) | async-done | bytes 4194320 | tf_op jit(solution)/shard_map/all_gather | solution.py:32
  189.6 14.4 %convolution_convert_fusion = bf16[1024,2048]{1,0:T(8,128)(2,1)} fusion(bf16[1024,2048]{1,0:T(8,128)(2,1)} %all-gather.5.cloned.1.call-done, bf16[1024,2048]{1,0:T(8,128)(2,1)} %bitcast.4, bf16[2048,1024]{1,0:T(8,128)(2,1)} %all-gather.3.cloned.1.call-done), kind=kOutput, calls=%fused_computation.1 | convolution fusion | flops 8595177472 | bytes 16777216 | tf_op jit(solution)/shard_map/dot_general | solution.py:34
  204.0 0.0 copy-start
  204.0 0.1 reduce-scatter.2.cloned.1.call-update
  204.1 40.5 %reduce-scatter.2.cloned.1.call-done = bf16[128,2048]{1,0:T(8,128)(2,1)} async-done(((bf16[1024,2048]{1,0:T(8,128)(2,1)}), bf16[128,2048]{1,0:T(8,128)(2,1)}) %reduce-scatter.2.cloned.1.call-update) | async-done | bytes 524304 | tf_op jit(solution)/shard_map/reduce_scatter | solution.py:33
  244.5 0.0 copy-done
  244.5 2.0 fusion.3
  (1 shorter events, 0.0 us)
Async XLA Ops:
  6.5 91.8 %all-gather.3.cloned.1.call-start = ((), (), s32[]{:S(2)}) async-start(), calls=%async_computation.2 | async-start | bytes 4456448 | tf_op jit(solution)/shard_map/all_gather | solution.py:29
  7.3 182.3 %all-gather.5.cloned.1.call-start = ((), (), s32[]{:S(2)}) async-start(), calls=%async_computation.3 | async-start | bytes 4456448 | tf_op jit(solution)/shard_map/all_gather | solution.py:32
  8.1 236.4 %reduce-scatter.2.cloned.1.call-start = ((), (), s32[]{:S(2)}) async-start(), calls=%async_computation.4 | async-start | bytes 4718592 | tf_op jit(solution)/shard_map/reduce_scatter | solution.py:33
  204.0 40.6 %copy-start = (bf16[128,2048]{1,0:T(8,128)(2,1)S(1)}, bf16[128,2048]{1,0:T(8,128)(2,1)}, u32[]{:S(2)}) copy-start(bf16[128,2048]{1,0:T(8,128)(2,1)} %param.4) | copy-start | bytes 1572868
Sparse Core Ops, SparseCore 0:
  9.1 89.1 all-gather.2
  100.1 89.5 all-gather.4
  204.2 40.3 reduce-scatter.1
where the time goes:
time: 253 us
  waiting for transfers between devices  166 us (66%)
  blocking collectives  54.2 us (21%)
  matrix products  14.4 us (6%)
  between operations  13.1 us (5%)
  other arithmetic  4.44 us (2%)
    all_gather x1, waiting for transfers between devices, local(): whole_out = lax.all_gather(w_out, 'fs', axis=1, tiled=True)  91.3 us
    all_to_all x1, blocking collectives, from_everyone(): return lax.all_to_all(copies, axis, split_axis=0, concat_axis=0, tiled=True)  54.2 us
    reduce_scatter x1, waiting for transfers between devices, local(): lax.psum_scatter(jnp.dot(hidden, whole_out, preferred_element_type=jnp.fl...  40.5 us
    all_gather x1, waiting for transfers between devices, local(): whole_in = lax.all_gather(w_in, 'fs', axis=0, tiled=True)  33 us
    dot_general x1, matrix products, local(): jnp.dot(hidden, whole_out, preferred_element_type=jnp.float32)  14.4 us
  transfers between devices with their start and end apart: 3, of which 3 were waited for; matrix products, arithmetic and copies ran while one was open for 1% of the time, Pallas kernels for 0%

commit v1 on v0

--- a/solution.py
+++ b/solution.py
@@ -4,6 +4,14 @@
 from jax.sharding import PartitionSpec as P
 
 EPS = 1e-06
+
+
+def meshes_supply(here_x, at_axis):
+    here_x = jnp.moveaxis(here_x, 0, at_axis)
+    later = here_x.shape
+    return here_x.reshape(
+        *later[:at_axis], later[at_axis] * later[at_axis + 1], *later[at_axis + 2 :]
+    )
 
 
 def from_everyone(shard, axis):
@@ -26,7 +34,19 @@
     xf = tokens.astype(jnp.float32)
     scale = lax.rsqrt(jnp.mean(xf * xf, axis=-1, keepdims=True) + EPS)
     normed = (xf * scale * norm_gain).astype(jnp.bfloat16)
-    whole_in = lax.all_gather(w_in, "fs", axis=0, tiled=True)
+    axis_len = lax.axis_size("fs")
+    queue = tuple(((jj, (jj + 1) % axis_len) for jj in range(axis_len)))
+    sides = tuple(((m, it) for it, m in queue))
+    left_arr, opened = ([], [])
+    for u in tuple(range(axis_len - 1)):
+        if u % 2 == 0:
+            left_arr.append(lax.ppermute(left_arr[-1] if left_arr else w_in, "fs", queue))
+        else:
+            opened.append(lax.ppermute(opened[-1] if opened else w_in, "fs", sides))
+    n_now = jnp.stack([*left_arr[::-1], w_in, *opened], 0)
+    shaped = lax.axis_index("fs") - len(left_arr)
+    n_now = n_now[(jnp.arange(axis_len) - shaped) % axis_len]
+    whole_in = meshes_supply(n_now, 0)
     pre = jnp.dot(collect(normed, "tp", 0), whole_in, preferred_element_type=jnp.float32)
     hidden = jnp.square(jax.nn.relu(pre)).astype(jnp.bfloat16)
     whole_out = lax.all_gather(w_out, "fs", axis=1, tiled=True)

time: 253 us -> 228 us (0.901)
  blocking collectives: 54.2 us -> 0 us
  starting transfers between devices: 0.13 us -> 35 us
  waiting for transfers between devices: 166 us -> 139 us
  local copies, waits for them, and re-layouts: 0.52 us -> 20.9 us
    all_gather x1, waiting for transfers between devices: 91.3 us -> 0.01 us  [local(): whole_out = lax.all_gather(w_out, 'fs', axis=1, tiled=True)]
    ppermute x0 -> x15, waiting for transfers between devices: none -> 66.9 us  [the longest x8 66.5 us: local(): lax.ppermute(left_arr[-1] if left_arr else w_in, 'fs', queue)]
    all_to_all x1 -> x0, blocking collectives: 54.2 us -> none  [from_everyone(): return lax.all_to_all(copies, axis, split_axis=0, concat_axis=0, tiled=True)]
    all_gather x1 -> x0, waiting for transfers between devices: 33 us -> none  [local(): whole_in = lax.all_gather(w_in, 'fs', axis=0, tiled=True)]
    ppermute x0 -> x15, starting transfers between devices: none -> 30.1 us  [the longest x7 20.3 us: local(): opened.append(lax.ppermute(opened[-1] if opened else w_in, 'fs', sides))]
    all_to_all x0 -> x1, waiting for transfers between devices: none -> 28 us  [from_everyone(): return lax.all_to_all(copies, axis, split_axis=0, concat_axis=0, tiled=True)]
    unnamed x2 -> x19, local copies, waits for them, and re-layouts: 0.01 us -> 12.7 us
    gather x0 -> x1, local copies, waits for them, and re-layouts: none -> 4.94 us  [local(): n_now = n_now[(jnp.arange(axis_len) - shaped) % axis_len]]
  transfers between devices with their start and end apart: 3 -> 18, of which waited for: 3 -> 11; matrix products, arithmetic and copies ran while one was open for 1% -> 10% of each run, Pallas kernels for 0% -> 0%
where the time goes in v1:
time: 228 us; the launch traced here: 227 us
  waiting for transfers between devices  139 us (61%)
  starting transfers between devices  35 us (15%)
  local copies, waits for them, and re-layouts  20.9 us (9%)
  matrix products  14.4 us (6%)
  between operations  13.5 us (6%)
  other arithmetic  4.45 us (2%)
    ppermute x8, waiting for transfers between devices, local(): lax.ppermute(left_arr[-1] if left_arr else w_in, 'fs', queue)  66.5 us
    reduce_scatter x1, waiting for transfers between devices, local(): lax.psum_scatter(jnp.dot(hidden, whole_out, preferred_element_type=jnp.fl...  43.1 us
    all_to_all x1, waiting for transfers between devices, from_everyone(): return lax.all_to_all(copies, axis, split_axis=0, concat_axis=0, tiled=True)  28 us
    ppermute x7, starting transfers between devices, local(): opened.append(lax.ppermute(opened[-1] if opened else w_in, 'fs', sides))  20.3 us
    dot_general x1, matrix products, local(): jnp.dot(hidden, whole_out, preferred_element_type=jnp.float32)  14.4 us
    unnamed x19, local copies, waits for them, and re-layouts  12.7 us
    ppermute x8, starting transfers between devices, local(): lax.ppermute(left_arr[-1] if left_arr else w_in, 'fs', queue)  9.81 us
    gather x1, local copies, waits for them, and re-layouts, local(): n_now = n_now[(jnp.arange(axis_len) - shaped) % axis_len]  4.94 us
  transfers between devices with their start and end apart: 18, of which 11 were waited for; matrix products, arithmetic and copies ran while one was open for 10% of the time, Pallas kernels for 0%

profile of v1, /device:TPU:40, one launch (start us, length us, event | category | flops | bytes accessed | tf_op | source)
XLA Modules:
  0.0 227.1 jit_solution(6045182194048862733)
XLA Ops:
  7.3 2.9 %collective-permute-start = (bf16[128,1024]{1,0:T(8,128)(2,1)}, bf16[128,1024]{1,0:T(8,128)(2,1)S(1)}, u32[]{:S(2)}, u32[]{:S(2)}) collective-permute-start(bf16[128,1024]{1,0:T(8,128)(2,1)} %param.6), channel_id=1, source_target_pairs={{0,8},{8,16},{16,24},{24,32},{32,40},{40,48},{48,56},{56,64},{64,7... | collective-permute-start | bytes 786440 | tf_op jit(solution)/shard_map/ppermute | solution.py:43
  10.2 26.2 %collective-permute-done = bf16[128,1024]{1,0:T(8,128)(2,1)S(1)} collective-permute-done((bf16[128,1024]{1,0:T(8,128)(2,1)}, bf16[128,1024]{1,0:T(8,128)(2,1)S(1)}, u32[]{:S(2)}, u32[]{:S(2)}) %collective-permute-start) | collective-permute-done | bytes 262176 | tf_op jit(solution)/shard_map/ppermute | solution.py:43
  36.4 3.2 %collective-permute-start.8 = (bf16[128,1024]{1,0:T(8,128)(2,1)}, bf16[128,1024]{1,0:T(8,128)(2,1)S(1)}, u32[]{:S(2)}, u32[]{:S(2)}) collective-permute-start(bf16[128,1024]{1,0:T(8,128)(2,1)} %param.6), channel_id=1, source_target_pairs={{8,0},{16,8},{24,16},{32,24},{40,32},{48,40},{56,48},{64,56},{72,6... | collective-permute-start | bytes 786440 | tf_op jit(solution)/shard_map/ppermute | solution.py:45
  39.6 8.3 %collective-permute-done.1 = bf16[128,1024]{1,0:T(8,128)(2,1)S(1)} collective-permute-done((bf16[128,1024]{1,0:T(8,128)(2,1)S(1)}, bf16[128,1024]{1,0:T(8,128)(2,1)S(1)}, u32[]{:S(2)}, u32[]{:S(2)}) %collective-permute-start.1) | collective-permute-done | bytes 262176 | tf_op jit(solution)/shard_map/ppermute | solution.py:43
  48.2 3.0 %collective-permute-start.9 = (bf16[128,1024]{1,0:T(8,128)(2,1)S(1)}, bf16[128,1024]{1,0:T(8,128)(2,1)S(1)}, u32[]{:S(2)}, u32[]{:S(2)}) collective-permute-start(bf16[128,1024]{1,0:T(8,128)(2,1)S(1)} %collective-permute-done.8), channel_id=1, source_target_pairs={{8,0},{16,8},{24,16},{32,24},{40,32},{48,40},{56,48},{64,56},{72,6... | collective-permute-start | bytes 786440 | tf_op jit(solution)/shard_map/ppermute | solution.py:45
  51.2 7.9 %collective-permute-done.2 = bf16[128,1024]{1,0:T(8,128)(2,1)S(1)} collective-permute-done((bf16[128,1024]{1,0:T(8,128)(2,1)S(1)}, bf16[128,1024]{1,0:T(8,128)(2,1)S(1)}, u32[]{:S(2)}, u32[]{:S(2)}) %collective-permute-start.2) | collective-permute-done | bytes 262176 | tf_op jit(solution)/shard_map/ppermute | solution.py:43
  62.4 6.7 %collective-permute-done.3 = bf16[128,1024]{1,0:T(8,128)(2,1)S(1)} collective-permute-done((bf16[128,1024]{1,0:T(8,128)(2,1)S(1)}, bf16[128,1024]{1,0:T(8,128)(2,1)S(1)}, u32[]{:S(2)}, u32[]{:S(2)}) %collective-permute-start.3) | collective-permute-done | bytes 262176 | tf_op jit(solution)/shard_map/ppermute | solution.py:43
  69.1 2.0 collective-permute-start.4
  71.2 3.7 %collective-permute-start.11 = (bf16[128,1024]{1,0:T(8,128)(2,1)S(1)}, bf16[128,1024]{1,0:T(8,128)(2,1)S(1)}, u32[]{:S(2)}, u32[]{:S(2)}) collective-permute-start(bf16[128,1024]{1,0:T(8,128)(2,1)S(1)} %collective-permute-done.10), channel_id=1, source_target_pairs={{8,0},{16,8},{24,16},{32,24},{40,32},{48,40},{56,48},{64,56},{72,6... | collective-permute-start | bytes 786440 | tf_op jit(solution)/shard_map/ppermute | solution.py:45
  74.9 4.3 %collective-permute-done.4 = bf16[128,1024]{1,0:T(8,128)(2,1)S(1)} collective-permute-done((bf16[128,1024]{1,0:T(8,128)(2,1)S(1)}, bf16[128,1024]{1,0:T(8,128)(2,1)S(1)}, u32[]{:S(2)}, u32[]{:S(2)}) %collective-permute-start.4) | collective-permute-done | bytes 262176 | tf_op jit(solution)/shard_map/ppermute | solution.py:43
  79.2 2.5 %collective-permute-start.5 = (bf16[128,1024]{1,0:T(8,128)(2,1)S(1)}, bf16[128,1024]{1,0:T(8,128)(2,1)S(1)}, u32[]{:S(2)}, u32[]{:S(2)}) collective-permute-start(bf16[128,1024]{1,0:T(8,128)(2,1)S(1)} %collective-permute-done.4), channel_id=1, source_target_pairs={{0,8},{8,16},{16,24},{24,32},{32,40},{40,48},{48,56},{56,64},{64,7... | collective-permute-start | bytes 786440 | tf_op jit(solution)/shard_map/ppermute | solution.py:43
  81.7 3.0 %collective-permute-start.12 = (bf16[128,1024]{1,0:T(8,128)(2,1)S(1)}, bf16[128,1024]{1,0:T(8,128)(2,1)S(1)}, u32[]{:S(2)}, u32[]{:S(2)}) collective-permute-start(bf16[128,1024]{1,0:T(8,128)(2,1)S(1)} %collective-permute-done.11), channel_id=1, source_target_pairs={{8,0},{16,8},{24,16},{32,24},{40,32},{48,40},{56,48},{64,56},{72,6... | collective-permute-start | bytes 786440 | tf_op jit(solution)/shard_map/ppermute | solution.py:45
  84.7 5.8 %collective-permute-done.5 = bf16[128,1024]{1,0:T(8,128)(2,1)S(1)} collective-permute-done((bf16[128,1024]{1,0:T(8,128)(2,1)S(1)}, bf16[128,1024]{1,0:T(8,128)(2,1)S(1)}, u32[]{:S(2)}, u32[]{:S(2)}) %collective-permute-start.5) | collective-permute-done | bytes 262176 | tf_op jit(solution)/shard_map/ppermute | solution.py:43
  92.6 2.5 %collective-permute-start.13 = (bf16[128,1024]{1,0:T(8,128)(2,1)S(1)}, bf16[128,1024]{1,0:T(8,128)(2,1)S(1)}, u32[]{:S(2)}, u32[]{:S(2)}) collective-permute-start(bf16[128,1024]{1,0:T(8,128)(2,1)S(1)} %collective-permute-done.12), channel_id=1, source_target_pairs={{8,0},{16,8},{24,16},{32,24},{40,32},{48,40},{56,48},{64,56},{72,6... | collective-permute-start | bytes 786440 | tf_op jit(solution)/shard_map/ppermute | solution.py:45
  95.1 7.2 %collective-permute-done.6 = bf16[128,1024]{1,0:T(8,128)(2,1)} collective-permute-done((bf16[128,1024]{1,0:T(8,128)(2,1)S(1)}, bf16[128,1024]{1,0:T(8,128)(2,1)}, u32[]{:S(2)}, u32[]{:S(2)}) %collective-permute-start.6) | collective-permute-done | bytes 262176 | tf_op jit(solution)/shard_map/ppermute | solution.py:43
  103.6 2.5 %broadcast_in_dim.2 = bf16[8,128,2048]{2,1,0:T(8,128)(2,1)} broadcast(bf16[128,2048]{1,0:T(8,128)(2,1)S(1)} %fusion.2), dimensions={1,2} | broadcast | bytes 4718592 | tf_op jit(solution)/shard_map/broadcast_in_dim | solution.py:18
  106.1 4.9 %all-to-all-start = ((bf16[8,128,2048]{2,1,0:T(8,128)(2,1)}), bf16[8,128,2048]{2,1,0:T(8,128)(2,1)}, u32[]{:S(2)}, u32[]{:S(2)}) async-start(bf16[8,128,2048]{2,1,0:T(8,128)(2,1)} %broadcast_in_dim.2), calls=%async_computation | async-start | bytes 8388608 | tf_op jit(solution)/shard_map/all_to_all | solution.py:19
  111.1 3.2 %collective-permute-start.14 = (bf16[128,1024]{1,0:T(8,128)(2,1)S(1)}, bf16[128,1024]{1,0:T(8,128)(2,1)S(1)}, u32[]{:S(2)}, u32[]{:S(2)}) collective-permute-start(bf16[128,1024]{1,0:T(8,128)(2,1)S(1)} %collective-permute-done.13), channel_id=1, source_target_pairs={{8,0},{16,8},{24,16},{32,24},{40,32},{48,40},{56,48},{64,56},{72,6... | collective-permute-start | bytes 786440 | tf_op jit(solution)/shard_map/ppermute | solution.py:45
  114.3 1.7 bitcast_dynamic-update-slice_fusion.15
  127.8 4.9 %gather_fusion = bf16[16,128,1024]{2,1,0:T(8,128)(2,1)} fusion(bf16[16,128,1024]{2,1,0:T(8,128)(2,1)} %bitcast_dynamic-update-slice_fusion, s32[1024]{0:T(1024)S(1)} %pad_clamp_fusion), kind=kCustom, calls=%fused_computation | custom fusion | bytes 8388672 | tf_op jit(solution)/shard_map/gather | solution.py:48
  132.7 28.0 %all-to-all-done = bf16[8,128,2048]{2,1,0:T(8,128)(2,1)} async-done(((bf16[8,128,2048]{2,1,0:T(8,128)(2,1)}), bf16[8,128,2048]{2,1,0:T(8,128)(2,1)}, u32[]{:S(2)}, u32[]{:S(2)}) %all-to-all-start) | async-done | bytes 4194336 | tf_op jit(solution)/shard_map/all_to_all | solution.py:19
  160.7 14.4 %convolution_convert_fusion = bf16[1024,2048]{1,0:T(8,128)(2,1)} fusion(bf16[1024,2048]{1,0:T(8,128)(2,1)} %all-gather.2.cloned.1.call-done, bf16[1024,2048]{1,0:T(8,128)(2,1)} %bitcast, bf16[2048,1024]{1,0:T(8,128)(2,1)} %bitcast.39), kind=kOutput, calls=%fused_computation.2 | convolution fusion | flops 8595177472 | bytes 16777216 | tf_op jit(solution)/shard_map/dot_general | solution.py:54
  175.2 43.1 %reduce-scatter.2.cloned.1.call-done = bf16[128,2048]{1,0:T(8,128)(2,1)} async-done(((bf16[1024,2048]{1,0:T(8,128)(2,1)}), bf16[128,2048]{1,0:T(8,128)(2,1)}) %reduce-scatter.2.cloned.1.call-update) | async-done | bytes 524304 | tf_op jit(solution)/shard_map/reduce_scatter | solution.py:53
  218.3 2.0 fusion.3
  (43 shorter events, 19.6 us)
Async XLA Ops:
  6.5 154.2 %all-gather.2.cloned.1.call-start = ((), (), s32[]{:S(2)}) async-start(), calls=%async_computation.2 | async-start | bytes 4456448 | tf_op jit(solution)/shard_map/all_gather | solution.py:52
  7.3 29.1 %collective-permute-start = (bf16[128,1024]{1,0:T(8,128)(2,1)}, bf16[128,1024]{1,0:T(8,128)(2,1)S(1)}, u32[]{:S(2)}, u32[]{:S(2)}) collective-permute-start(bf16[128,1024]{1,0:T(8,128)(2,1)} %param.6), channel_id=1, source_target_pairs={{0,8},{8,16},{16,24},{24,32},{32,40},{40,48},{48,56},{56,64},{64,7... | collective-permute-start | bytes 786440 | tf_op jit(solution)/shard_map/ppermute | solution.py:43
  36.4 11.6 %collective-permute-start.1 = (bf16[128,1024]{1,0:T(8,128)(2,1)S(1)}, bf16[128,1024]{1,0:T(8,128)(2,1)S(1)}, u32[]{:S(2)}, u32[]{:S(2)}) collective-permute-start(bf16[128,1024]{1,0:T(8,128)(2,1)S(1)} %collective-permute-done), channel_id=1, source_target_pairs={{0,8},{8,16},{16,24},{24,32},{32,40},{40,48},{48,56},{56,64},{64,7... | collective-permute-start | bytes 786440 | tf_op jit(solution)/shard_map/ppermute | solution.py:43
  36.4 11.8 %collective-permute-start.8 = (bf16[128,1024]{1,0:T(8,128)(2,1)}, bf16[128,1024]{1,0:T(8,128)(2,1)S(1)}, u32[]{:S(2)}, u32[]{:S(2)}) collective-permute-start(bf16[128,1024]{1,0:T(8,128)(2,1)} %param.6), channel_id=1, source_target_pairs={{8,0},{16,8},{24,16},{32,24},{40,32},{48,40},{56,48},{64,56},{72,6... | collective-permute-start | bytes 786440 | tf_op jit(solution)/shard_map/ppermute | solution.py:45
  48.0 11.2 %collective-permute-start.2 = (bf16[128,1024]{1,0:T(8,128)(2,1)S(1)}, bf16[128,1024]{1,0:T(8,128)(2,1)S(1)}, u32[]{:S(2)}, u32[]{:S(2)}) collective-permute-start(bf16[128,1024]{1,0:T(8,128)(2,1)S(1)} %collective-permute-done.1), channel_id=1, source_target_pairs={{0,8},{8,16},{16,24},{24,32},{32,40},{40,48},{48,56},{56,64},{64,7... | collective-permute-start | bytes 786440 | tf_op jit(solution)/shard_map/ppermute | solution.py:43
  48.2 12.5 %collective-permute-start.9 = (bf16[128,1024]{1,0:T(8,128)(2,1)S(1)}, bf16[128,1024]{1,0:T(8,128)(2,1)S(1)}, u32[]{:S(2)}, u32[]{:S(2)}) collective-permute-start(bf16[128,1024]{1,0:T(8,128)(2,1)S(1)} %collective-permute-done.8), channel_id=1, source_target_pairs={{8,0},{16,8},{24,16},{32,24},{40,32},{48,40},{56,48},{64,56},{72,6... | collective-permute-start | bytes 786440 | tf_op jit(solution)/shard_map/ppermute | solution.py:45
  59.1 10.0 %collective-permute-start.3 = (bf16[128,1024]{1,0:T(8,128)(2,1)S(1)}, bf16[128,1024]{1,0:T(8,128)(2,1)S(1)}, u32[]{:S(2)}, u32[]{:S(2)}) collective-permute-start(bf16[128,1024]{1,0:T(8,128)(2,1)S(1)} %collective-permute-done.2), channel_id=1, source_target_pairs={{0,8},{8,16},{16,24},{24,32},{32,40},{40,48},{48,56},{56,64},{64,7... | collective-permute-start | bytes 786440 | tf_op jit(solution)/shard_map/ppermute | solution.py:43
  60.7 10.5 %collective-permute-start.10 = (bf16[128,1024]{1,0:T(8,128)(2,1)S(1)}, bf16[128,1024]{1,0:T(8,128)(2,1)S(1)}, u32[]{:S(2)}, u32[]{:S(2)}) collective-permute-start(bf16[128,1024]{1,0:T(8,128)(2,1)S(1)} %collective-permute-done.9), channel_id=1, source_target_pairs={{8,0},{16,8},{24,16},{32,24},{40,32},{48,40},{56,48},{64,56},{72,6... | collective-permute-start | bytes 786440 | tf_op jit(solution)/shard_map/ppermute | solution.py:45
  69.1 10.1 %collective-permute-start.4 = (bf16[128,1024]{1,0:T(8,128)(2,1)S(1)}, bf16[128,1024]{1,0:T(8,128)(2,1)S(1)}, u32[]{:S(2)}, u32[]{:S(2)}) collective-permute-start(bf16[128,1024]{1,0:T(8,128)(2,1)S(1)} %collective-permute-done.3), channel_id=1, source_target_pairs={{0,8},{8,16},{16,24},{24,32},{32,40},{40,48},{48,56},{56,64},{64,7... | collective-permute-start | bytes 786440 | tf_op jit(solution)/shard_map/ppermute | solution.py:43
  71.2 10.5 %collective-permute-start.11 = (bf16[128,1024]{1,0:T(8,128)(2,1)S(1)}, bf16[128,1024]{1,0:T(8,128)(2,1)S(1)}, u32[]{:S(2)}, u32[]{:S(2)}) collective-permute-start(bf16[128,1024]{1,0:T(8,128)(2,1)S(1)} %collective-permute-done.10), channel_id=1, source_target_pairs={{8,0},{16,8},{24,16},{32,24},{40,32},{48,40},{56,48},{64,56},{72,6... | collective-permute-start | bytes 786440 | tf_op jit(solution)/shard_map/ppermute | solution.py:45
  79.2 11.3 %collective-permute-start.5 = (bf16[128,1024]{1,0:T(8,128)(2,1)S(1)}, bf16[128,1024]{1,0:T(8,128)(2,1)S(1)}, u32[]{:S(2)}, u32[]{:S(2)}) collective-permute-start(bf16[128,1024]{1,0:T(8,128)(2,1)S(1)} %collective-permute-done.4), channel_id=1, source_target_pairs={{0,8},{8,16},{16,24},{24,32},{32,40},{40,48},{48,56},{56,64},{64,7... | collective-permute-start | bytes 786440 | tf_op jit(solution)/shard_map/ppermute | solution.py:43
  81.7 10.8 %collective-permute-start.12 = (bf16[128,1024]{1,0:T(8,128)(2,1)S(1)}, bf16[128,1024]{1,0:T(8,128)(2,1)S(1)}, u32[]{:S(2)}, u32[]{:S(2)}) collective-permute-start(bf16[128,1024]{1,0:T(8,128)(2,1)S(1)} %collective-permute-done.11), channel_id=1, source_target_pairs={{8,0},{16,8},{24,16},{32,24},{40,32},{48,40},{56,48},{64,56},{72,6... | collective-permute-start | bytes 786440 | tf_op jit(solution)/shard_map/ppermute | solution.py:45
  90.5 11.8 %collective-permute-start.6 = (bf16[128,1024]{1,0:T(8,128)(2,1)S(1)}, bf16[128,1024]{1,0:T(8,128)(2,1)}, u32[]{:S(2)}, u32[]{:S(2)}) collective-permute-start(bf16[128,1024]{1,0:T(8,128)(2,1)S(1)} %collective-permute-done.5), channel_id=1, source_target_pairs={{0,8},{8,16},{16,24},{24,32},{32,40},{40,48},{48,56},{56,64},{64,7... | collective-permute-start | bytes 786440 | tf_op jit(solution)/shard_map/ppermute | solution.py:43
  92.6 18.5 %collective-permute-start.13 = (bf16[128,1024]{1,0:T(8,128)(2,1)S(1)}, bf16[128,1024]{1,0:T(8,128)(2,1)S(1)}, u32[]{:S(2)}, u32[]{:S(2)}) collective-permute-start(bf16[128,1024]{1,0:T(8,128)(2,1)S(1)} %collective-permute-done.12), channel_id=1, source_target_pairs={{8,0},{16,8},{24,16},{32,24},{40,32},{48,40},{56,48},{64,56},{72,6... | collective-permute-start | bytes 786440 | tf_op jit(solution)/shard_map/ppermute | solution.py:45
  102.3 12.0 %collective-permute-start.7 = (bf16[128,1024]{1,0:T(8,128)(2,1)}, bf16[128,1024]{1,0:T(8,128)(2,1)}, u32[]{:S(2)}, u32[]{:S(2)}) collective-permute-start(bf16[128,1024]{1,0:T(8,128)(2,1)} %collective-permute-done.6), channel_id=1, source_target_pairs={{0,8},{8,16},{16,24},{24,32},{32,40},{40,48},{48,56},{56,64},{64,7... | collective-permute-start | bytes 786440 | tf_op jit(solution)/shard_map/ppermute | solution.py:43
  106.1 54.6 %all-to-all-start = ((bf16[8,128,2048]{2,1,0:T(8,128)(2,1)}), bf16[8,128,2048]{2,1,0:T(8,128)(2,1)}, u32[]{:S(2)}, u32[]{:S(2)}) async-start(bf16[8,128,2048]{2,1,0:T(8,128)(2,1)} %broadcast_in_dim.2), calls=%async_computation | async-start | bytes 8388608 | tf_op jit(solution)/shard_map/all_to_all | solution.py:19
  111.0 11.0 %copy-start.1 = (bf16[128,1024]{1,0:T(8,128)(2,1)S(1)}, bf16[128,1024]{1,0:T(8,128)(2,1)}, u32[]{:S(2)}) copy-start(bf16[128,1024]{1,0:T(8,128)(2,1)} %param.6) | copy-start | bytes 786436
  111.0 107.3 %reduce-scatter.2.cloned.1.call-start = ((), (), s32[]{:S(2)}) async-start(), calls=%async_computation.3 | async-start | bytes 4718592 | tf_op jit(solution)/shard_map/reduce_scatter | solution.py:53
  111.1 15.9 %collective-permute-start.14 = (bf16[128,1024]{1,0:T(8,128)(2,1)S(1)}, bf16[128,1024]{1,0:T(8,128)(2,1)S(1)}, u32[]{:S(2)}, u32[]{:S(2)}) collective-permute-start(bf16[128,1024]{1,0:T(8,128)(2,1)S(1)} %collective-permute-done.13), channel_id=1, source_target_pairs={{8,0},{16,8},{24,16},{32,24},{40,32},{48,40},{56,48},{64,56},{72,6... | collective-permute-start | bytes 786440 | tf_op jit(solution)/shard_map/ppermute | solution.py:45
  175.1 43.2 %copy-start = (bf16[128,2048]{1,0:T(8,128)(2,1)S(1)}, bf16[128,2048]{1,0:T(8,128)(2,1)}, u32[]{:S(2)}) copy-start(bf16[128,2048]{1,0:T(8,128)(2,1)} %param.4) | copy-start | bytes 1572868
Sparse Core Ops, SparseCore 0:
  9.1 125.3 all-gather.1
  175.3 42.9 reduce-scatter.1
